TPU v7x, 512 devices: a 8x2x16 block of a 8x8x16 slice. The times are simulated.
512 devices in a mesh: grp: 2 (over y), sp: 32 (over z, core), tp: 8 (over x).
Axes of the slice: x: 8, y: 2, z: 16, core: 2. Of those that a mesh axis runs over, the one named last changes fastest.
The devices are a block of a 8x8x16 slice.
Arguments:
- residual: bfloat16 [16384, 2048], P(('grp', 'sp')), parts along dimension 0, may hold values from -34 to 34
- queries: bfloat16 [16384, 1024], P(('grp', 'sp'), 'tp'), parts along dimension 0, may hold values from -400 to 400
- keys: bfloat16 [16384, 512], P(('grp', 'sp'), 'tp'), parts along dimension 0, may hold values from -8 to 8
- values: bfloat16 [16384, 512], P(('grp', 'sp'), 'tp'), parts along dimension 0, may hold values from -6 to 6
- segments: int32 [16384], P(('grp', 'sp')), parts along dimension 0, may hold values from 0 to 16, never falling along the last dimension, each value on 1 to 768 neighbouring positions
- routes: int32 [16384, 2], P(('grp', 'sp')), parts along dimension 0, may hold values from 0 to 31, all different within a row; in each aligned block of 256 rows (0 to 255, 256 to 511, ...) at most 32 rows name the same one
- route_weight: float32 [16384, 2], P(('grp', 'sp')), parts along dimension 0, may hold values from 0.3 to 3
- sinks: float32 [16], P('tp'), may hold values from 1 to 6
- out_weight: bfloat16 [1024, 2048], P('tp'), may hold values from -1 to 1
- norm_gain: float32 [2048], replicated, may hold values from 0.1 to 1.9
- expert_gate: bfloat16 [32, 2048, 1024], P('sp', None, 'tp'), may hold values from -0.125 to 0.125
- expert_up: bfloat16 [32, 2048, 1024], P('sp', None, 'tp'), may hold values from -0.125 to 0.125
- expert_down: bfloat16 [32, 1024, 2048], P('sp', None, 'tp'), may hold values from -0.1875 to 0.1875
- shared_gate: bfloat16 [2048, 1024], P(None, 'tp'), may hold values from -0.125 to 0.125
- shared_up: bfloat16 [2048, 1024], P(None, 'tp'), may hold values from -0.125 to 0.125
- shared_down: bfloat16 [1024, 2048], P(None, 'tp'), may hold values from -0.1875 to 0.1875
Outputs:
- mixed: bfloat16 [16384, 2048], P(('grp', 'sp'), 'tp'), parts along dimension 0
There are 2 independent parts, one for each index of `grp`. A program takes and returns all parts, laid end to end along the dimension named above; an argument that names none is the same for every part. Nothing has to cross between parts.
Inputs may be any that keep to these rules, and one draw needn't show every extreme that they name: `routes`: each row names 2 different experts. In the rows of one device no expert is named by more than 32 rows, and in some device's rows an expert is named by exactly 32. `segments`: document numbers never fall along the positions; every document spans 1 to 768 positions and one spans exactly 768.
All inputs are finite; a program needn't handle non-finite values.
Results may differ from a plain program's by a relative error of at most 0.0065.
Values may be sent and summed in bfloat16 or wider, within the bound.
A program may use at most 64 MiB of HBM per device.

v0:
```python
import jax
import jax.numpy as jnp
from jax import lax
from jax.sharding import Mesh
from jax.sharding import PartitionSpec as P

HEAD_DIM = 64
WINDOW = 128
SP = ("sp_0", "sp_1")
GRP_SP = ("grp", "sp_0", "sp_1")
epsilon = 1e-06


def passed_along(value, axis, steps):
    count = lax.axis_size(axis)
    leading, last = (max(0, -steps), min(count, count - steps))
    return lax.ppermute(value, axis, [(source, source + steps) for source in range(leading, last)])


def split_up(array, dim, size):
    shape = array.shape
    blocks = array.reshape(*shape[:dim], size, shape[dim] // size, *shape[dim + 1 :])
    return jnp.moveaxis(blocks, dim, 0)


def sent_and_summed(array, axis, dim):
    size = lax.axis_size(axis)
    blocks = lax.all_to_all(split_up(array, dim, size), axis, 0, 0, tiled=True)
    return jnp.sum(blocks.astype(jnp.float32), axis=0)


def sent_to_all(array, axis):
    size = lax.axis_size(axis)
    return lax.all_to_all(
        jnp.broadcast_to(array[None], (size, *array.shape)), axis, 0, 0, tiled=True
    )


def in_order(blocks, dim):
    blocks = jnp.moveaxis(blocks, 0, dim)
    shape = blocks.shape
    return blocks.reshape(*shape[:dim], shape[dim] * shape[dim + 1], *shape[dim + 2 :])


def collect(array, axis, dim):
    blocks = sent_to_all(array, axis)
    return in_order(blocks, dim)


def moved_by_axis(blocks, axes, order):
    shape = [lax.axis_size(a) for a in axes]
    blocks = blocks.reshape(*shape, *blocks.shape[1:])
    for k in order:
        blocks = lax.all_to_all(blocks, axes[k], split_axis=k, concat_axis=k, tiled=True)
    return blocks.reshape(-1, *blocks.shape[len(axes) :])


def two_step_exchange(array, groups, order, split_dim, concat_dim):
    size = lax.axis_size(groups[0]) * lax.axis_size(groups[1])
    blocks = split_up(array, split_dim, size)
    return in_order(moved_by_axis(blocks, groups, order), concat_dim)


def sent_together(arrays, axis, dim, along):
    ends, at = ([], 0)
    for a in arrays[:-1]:
        at += a.shape[along]
        ends.append(at)
    both = jnp.concatenate(arrays, axis=along)
    return tuple(jnp.split(lax.all_gather(both, axis, axis=dim, tiled=True), ends, axis=along))


def banded(prev_rows, own_rows, window_len):
    blocks = own_rows.shape[0] // window_len
    joined = jnp.concatenate([prev_rows, own_rows], axis=0)
    shaped = joined.reshape((blocks + 1, window_len) + own_rows.shape[1:])
    return jnp.concatenate([shaped[:-1], shaped[1:]], axis=1)


def shards(
    residual,
    queries,
    keys,
    values,
    segments,
    routes,
    route_weight,
    sinks,
    out_weight,
    norm_gain,
    expert_gate,
    expert_up,
    expert_down,
    shared_gate,
    shared_up,
    shared_down,
):
    rows_here = residual.shape[0]
    model_width = residual.shape[1]
    tp_count = lax.axis_size("tp")
    tp_index = lax.axis_index("tp")
    head_local = queries.shape[1] // HEAD_DIM
    kv_local = keys.shape[1] // HEAD_DIM
    group_size = head_local // kv_local
    window_len = WINDOW
    blocks = rows_here // window_len
    own_marks = (segments % 256 + 1).astype(jnp.bfloat16)
    prev_keys, prev_values, prev_marks = passed_along(
        (
            keys[rows_here - window_len :],
            values[rows_here - window_len :],
            own_marks[rows_here - window_len :],
        ),
        SP,
        1,
    )
    key_band = banded(prev_keys, keys, window_len).reshape(
        blocks, 2 * window_len, kv_local, HEAD_DIM
    )
    value_band = banded(prev_values, values, window_len).reshape(
        blocks, 2 * window_len, kv_local, HEAD_DIM
    )
    mark_band = banded(prev_marks, own_marks, window_len).astype(jnp.float32)
    query_marks = own_marks.reshape(blocks, window_len).astype(jnp.float32)
    query_blocks = queries.reshape(blocks, window_len, kv_local, group_size, HEAD_DIM)
    scores = jnp.einsum(
        "nqhgd,nkhd->nhgqk", query_blocks, key_band, preferred_element_type=jnp.float32
    ) * HEAD_DIM ** (-0.5)
    offsets = jnp.arange(window_len)[:, None] + window_len - jnp.arange(2 * window_len)[None, :]
    allowed = (
        (offsets >= 0) & (offsets < window_len) & (query_marks[:, :, None] == mark_band[:, None, :])
    )
    sink_logits = sinks.reshape(kv_local, group_size)[None, :, :, None]
    masked = jnp.where(allowed[:, None, None], scores, -jnp.inf)
    top_score = jnp.maximum(jnp.max(masked, axis=-1), sink_logits)
    exp_terms = jnp.where(allowed[:, None, None], jnp.exp(scores - top_score[..., None]), 0.0)
    denominator = jnp.sum(exp_terms, axis=-1) + jnp.exp(sink_logits - top_score)
    probabilities = (exp_terms / denominator[..., None]).astype(jnp.bfloat16)
    attended = jnp.einsum(
        "nhgqk,nkhd->nqhgd", probabilities, value_band, preferred_element_type=jnp.float32
    )
    attended = attended.astype(jnp.bfloat16).reshape(rows_here, head_local * HEAD_DIM)
    partial_value = jnp.dot(attended, out_weight, preferred_element_type=jnp.float32)
    col_width = model_width // tp_count
    col_start = tp_index * col_width
    share_sum = sent_and_summed(partial_value.astype(jnp.bfloat16), "tp", 1)
    residual_cols = lax.dynamic_slice_in_dim(residual, col_start, col_width, 1)
    updated_cols = (residual_cols.astype(jnp.float32) + share_sum).astype(jnp.bfloat16)
    cols_f32 = updated_cols.astype(jnp.float32)
    squares = lax.psum(jnp.sum(cols_f32 * cols_f32, axis=-1), "tp")
    inv_rms = lax.rsqrt(squares / model_width + epsilon)
    gain_cols = lax.dynamic_slice_in_dim(norm_gain, col_start, col_width, 0)
    normed_cols = (cols_f32 * inv_rms[:, None] * gain_cols).astype(jnp.bfloat16)
    normed = collect(normed_cols, "tp", 1)
    shared_pre = jnp.dot(normed, shared_gate, preferred_element_type=jnp.float32)
    shared_lin = jnp.dot(normed, shared_up, preferred_element_type=jnp.float32)
    shared_act = (jax.nn.silu(shared_pre) * shared_lin).astype(jnp.bfloat16)
    top_count = routes.shape[1]
    experts = lax.axis_size(SP)
    capacity = 2 * rows_here * top_count // experts
    flat_ids = routes.reshape(-1)
    one_hot = (flat_ids[:, None] == jnp.arange(experts, dtype=jnp.int32)[None, :]).astype(jnp.int32)
    rank_in = jnp.cumsum(one_hot, axis=0) - one_hot
    slot_dest = flat_ids * capacity + jnp.sum(rank_in * one_hot, axis=1)
    token_of = jnp.arange(rows_here * top_count, dtype=jnp.int32) // top_count
    slot_token = jnp.full((experts * capacity,), -1, jnp.int32).at[slot_dest].set(token_of)
    filled = slot_token >= 0
    safe_token = jnp.where(filled, slot_token, 0)
    outgoing = jnp.where(filled[:, None], normed_cols[safe_token], jnp.zeros((), jnp.bfloat16))
    pieces = two_step_exchange(
        outgoing.reshape(experts, capacity, col_width), ("sp_0", "sp_1"), (1, 0), 0, 0
    )
    arrived = lax.all_gather(pieces, "tp", axis=2, tiled=True)
    expert_rows = arrived.reshape(-1, model_width)
    gate_pre = jnp.dot(expert_rows, expert_gate[0], preferred_element_type=jnp.float32)
    up_lin = jnp.dot(expert_rows, expert_up[0], preferred_element_type=jnp.float32)
    expert_act = (jax.nn.silu(gate_pre) * up_lin).astype(jnp.bfloat16)
    gathered_expert, gathered_shared = sent_together((expert_act, shared_act), "tp", 1, 0)
    expert_out = jnp.dot(
        gathered_expert, expert_down[0], preferred_element_type=jnp.float32
    ).astype(jnp.bfloat16)
    returned = lax.all_to_all(
        expert_out.reshape(experts, capacity, col_width),
        SP,
        split_axis=0,
        concat_axis=0,
        tiled=True,
    )
    returned = returned.reshape(experts * capacity, col_width)
    picked = returned[slot_dest].astype(jnp.float32).reshape(rows_here, top_count, col_width)
    routed = jnp.sum(picked * route_weight[:, :, None], axis=1)
    shared_cols = jnp.dot(gathered_shared, shared_down, preferred_element_type=jnp.float32)
    return (updated_cols.astype(jnp.float32) + shared_cols + routed).astype(jnp.bfloat16)


def solution(mesh):
    torus = Mesh(
        mesh.devices.reshape(mesh.shape["grp"], 16, 2, mesh.shape["tp"]),
        ("grp", "sp_0", "sp_1", "tp"),
    )
    in_specs = (
        P(GRP_SP, None),
        P(GRP_SP, "tp"),
        P(GRP_SP, "tp"),
        P(GRP_SP, "tp"),
        P(GRP_SP),
        P(GRP_SP, None),
        P(GRP_SP, None),
        P("tp"),
        P("tp", None),
        P(),
        P(SP, None, "tp"),
        P(SP, None, "tp"),
        P(SP, None, "tp"),
        P(None, "tp"),
        P(None, "tp"),
        P(None, "tp"),
    )
    out_specs = P(GRP_SP, "tp")
    return jax.shard_map(
        shards, mesh=torus, in_specs=in_specs, out_specs=out_specs, check_vma=False
    )
```

profile of v0, /device:TPU:65, one launch (start us, length us, event | category | flops | bytes accessed | tf_op | source)
XLA Modules:
  0.0 356.7 jit_solution(9728244078039882902)
XLA Ops:
  6.6 0.7 bitcast_convert_fusion
  7.3 7.1 %collective-permute-start.1 = (bf16[128]{0:T(256)(128)(2,1)S(1)}, bf16[128]{0:T(256)(128)(2,1)S(1)}, u32[]{:S(2)}, u32[]{:S(2)}) collective-permute-start(bf16[128]{0:T(256)(128)(2,1)S(1)} %slice.57), channel_id=1, source_target_pairs={{0,8},{8,16},{16,24},{24,32},{32,40},{40,48},{48,56},{56,64},{64,7... | collective-permute-start | bytes 776 | tf_op jit(solution)/shard_map/ppermute | solution.py:17
  14.4 0.7 slice.60
  15.1 1.9 collective-permute-start.2
  17.0 0.7 slice.53
  17.8 6.1 %collective-permute-start = (bf16[128,64]{0,1:T(8,128)(2,1)S(1)}, bf16[128,64]{0,1:T(8,128)(2,1)S(1)}, u32[]{:S(2)}, u32[]{:S(2)}) collective-permute-start(bf16[128,64]{0,1:T(8,128)(2,1)S(1)} %slice.53), channel_id=1, source_target_pairs={{0,8},{8,16},{16,24},{24,32},{32,40},{40,48},{48,56},{56,64},{64,7... | collective-permute-start | bytes 49160 | tf_op jit(solution)/shard_map/ppermute | solution.py:17
  23.9 0.8 copy_bitcast_fusion
  24.7 0.8 copy_bitcast_fusion.2
  25.5 0.9 reshape.250
  26.4 24.3 %collective-permute-done.1 = bf16[128]{0:T(256)(128)(2,1)S(1)} collective-permute-done((bf16[128]{0:T(256)(128)(2,1)S(1)}, bf16[128]{0:T(256)(128)(2,1)S(1)}, u32[]{:S(2)}, u32[]{:S(2)}) %collective-permute-start.1) | collective-permute-done | bytes 288 | tf_op jit(solution)/shard_map/ppermute | solution.py:17
  50.7 0.1 compare_and_fusion
  50.8 1.9 collective-permute-done.2
  52.7 0.7 copy_bitcast_fusion.1
  53.5 0.3 select_reduce_fusion
  53.7 0.7 broadcast_maximum_fusion
  54.5 0.1 fusion.16
  54.6 0.7 exponential_add_fusion
  55.3 0.7 copy_bitcast_fusion.3
  56.1 0.3 fusion.10
  56.3 0.1 copy.41
  56.4 0.5 convolution_convert_fusion
  56.9 1.1 copy.79
  57.9 3.8 %all-to-all-start = ((bf16[8,256,256]{2,1,0:T(8,128)(2,1)}), bf16[8,256,256]{2,1,0:T(8,128)(2,1)S(1)}, u32[]{:S(2)}, u32[]{:S(2)}) async-start(bf16[8,256,256]{2,1,0:T(8,128)(2,1)} %bitcast.106), calls=%async_computation | async-start | bytes 2097152 | tf_op jit(solution)/shard_map/all_to_all | solution.py:28
  61.7 0.1 all-gather.3.cloned.1.call-start
  61.8 0.1 copy.44
  61.9 0.1 eq.47
  62.1 0.1 eq.51
  62.2 0.1 copy.43
  62.4 0.1 mul.82
  62.5 1.2 reduce-window.6
  63.7 0.2 slice_reduce_fusion
  64.0 0.1 fusion.29
  64.1 2.4 scatter_custom_fusion
  66.6 0.1 broadcast_in_dim.66
  66.7 0.8 dynamic_slice.7
  67.4 19.8 %all-to-all-done = bf16[8,256,256]{2,1,0:T(8,128)(2,1)S(1)} async-done(((bf16[8,256,256]{2,1,0:T(8,128)(2,1)}), bf16[8,256,256]{2,1,0:T(8,128)(2,1)S(1)}, u32[]{:S(2)}, u32[]{:S(2)}) %all-to-all-start) | async-done | bytes 1048608 | tf_op jit(solution)/shard_map/all_to_all | solution.py:28
  87.2 0.1 convert_reduce_fusion
  87.4 1.0 fusion.17
  88.4 11.1 %psum.7 = f32[256]{0:T(256)S(1)} all-reduce(f32[256]{0:T(256)S(1)} %get-tuple-element.5), channel_id=1, replica_groups=mesh['grp'=2,'sp_0'=16,'sp_1'=2,'tp'=8] {'tp'}, use_global_device_ids=true, to_apply=%region_8.9 | all-reduce | flops 256 | bytes 2048 | tf_op jit(solution)/shard_map/psum | solution.py:150
  99.5 0.1 fusion.19
  99.6 3.9 %gather_fusion = bf16[1024,256]{1,0:T(8,128)(2,1)S(1)} fusion(bf16[256,256]{1,0:T(8,128)(2,1)S(1)} %fusion.19, s32[1024]{0:T(1024)S(1)} %fusion.37), kind=kCustom, calls=%fused_computation | custom fusion | bytes 1052672 | tf_op jit(solution)/shard_map/gather | solution.py:169
  103.5 0.2 copy_select_fusion
  103.8 11.5 %all_to_all.25 = bf16[16,2,1,32,256]{4,3,0,2,1:T(8,128)(2,1)S(1)} all-to-all(bf16[16,2,1,32,256]{4,3,0,2,1:T(8,128)(2,1)S(1)} %copy_select_fusion), channel_id=1, replica_groups=mesh['grp'=2,'sp_0'=16,'sp_1'=2,'tp'=8] {'sp_1'}, dimensions={1} | all-to-all | bytes 1048576 | tf_op jit(solution)/shard_map/all_to_all | solution.py:54
  115.3 36.5 %all_to_all.26 = bf16[16,2,1,32,256]{4,3,1,2,0:T(8,128)(2,1)} all-to-all(bf16[16,2,1,32,256]{4,3,1,2,0:T(8,128)(2,1)S(1)} %copy.49), channel_id=1, replica_groups=mesh['grp'=2,'sp_0'=16,'sp_1'=2,'tp'=8] {'sp_0'}, dimensions={0} | all-to-all | bytes 1048576 | tf_op jit(solution)/shard_map/all_to_all | solution.py:54
  151.8 0.1 all-gather.3.cloned.1.call-update
  151.9 0.1 all-gather.5.cloned.1.call-start
  152.0 0.1 copy.50
  152.1 0.1 broadcast_in_dim.70
  152.2 24.5 %all_to_all.27 = bf16[8,256,256]{1,2,0:T(8,128)(2,1)S(1)} all-to-all(bf16[8,256,256]{1,2,0:T(8,128)(2,1)S(1)} %broadcast_in_dim.70), channel_id=1, replica_groups=mesh['grp'=2,'sp_0'=16,'sp_1'=2,'tp'=8] {'tp'}, dimensions={0} | all-to-all | bytes 2097152 | tf_op jit(solution)/shard_map/all_to_all | solution.py:34
  176.6 0.5 fusion.50
  177.1 0.5 fusion.9
  177.6 47.7 %all-gather.3.cloned.1.call-done = bf16[32,32,2048]{2,1,0:T(8,128)(2,1)} async-done(((bf16[32,32,256]{2,1,0:T(8,128)(2,1)}), bf16[32,32,2048]{2,1,0:T(8,128)(2,1)}) %all-gather.3.cloned.1.call-update) | async-done | bytes 4194320 | tf_op jit(solution)/shard_map/all_gather | solution.py:173
  225.3 3.6 %fusion.14 = f32[1024,128]{1,0:T(8,128)S(1)} fusion(bf16[1024,2048]{1,0:T(8,128)(2,1)} %bitcast.108, bf16[1,2048,128]{2,1,0:T(8,128)(2,1)S(1)} %copy-done.2), kind=kOutput, calls=%fused_computation.23 | convolution fusion | flops 536870912 | bytes 5242880 | tf_op jit(solution)/shard_map/dot_general | solution.py:175
  229.0 1.2 fusion.6
  230.2 0.7 pad_maximum_fusion
  231.0 59.2 %all-gather.5.cloned.1.call-done = bf16[1280,1024]{1,0:T(8,128)(2,1)} async-done(((bf16[1280,128]{1,0:T(8,128)(2,1)}), bf16[1280,1024]{1,0:T(8,128)(2,1)}) %all-gather.5.cloned.1.call-update) | async-done | bytes 2621456 | tf_op jit(solution)/shard_map/all_gather | solution.py:70
  290.2 3.1 fusion.2
  293.3 18.3 %all-to-all-start.4 = ((bf16[32,32,256]{2,1,0:T(8,128)(2,1)}), bf16[32,32,256]{2,1,0:T(8,128)(2,1)S(1)}, u32[]{:S(2)}, u32[]{:S(2)}) async-start(bf16[32,32,256]{2,1,0:T(8,128)(2,1)} %bitcast.25), calls=%async_computation.4 | async-start | bytes 1048576 | tf_op jit(solution)/shard_map/all_to_all | solution.py:182
  311.7 0.1 copy.51
  311.8 33.1 %all-to-all-done.4 = bf16[32,32,256]{2,1,0:T(8,128)(2,1)S(1)} async-done(((bf16[32,32,256]{2,1,0:T(8,128)(2,1)}), bf16[32,32,256]{2,1,0:T(8,128)(2,1)S(1)}, u32[]{:S(2)}, u32[]{:S(2)}) %all-to-all-start.4) | async-done | bytes 524320 | tf_op jit(solution)/shard_map/all_to_all | solution.py:182
  344.9 1.9 gather_fusion.1
  346.9 0.3 reshape.222
  347.2 0.7 multiply_reduce_fusion
  347.9 2.0 fusion.8
  (40 shorter events, 0.3 us)
Async XLA Ops:
  6.5 49.8 %copy-start = (bf16[128,2048]{1,0:T(8,128)(2,1)S(1)}, bf16[128,2048]{1,0:T(8,128)(2,1)}, u32[]{:S(2)}) copy-start(bf16[128,2048]{1,0:T(8,128)(2,1)} %param.24) | copy-start | bytes 1572868
  7.3 43.4 %collective-permute-start.1 = (bf16[128]{0:T(256)(128)(2,1)S(1)}, bf16[128]{0:T(256)(128)(2,1)S(1)}, u32[]{:S(2)}, u32[]{:S(2)}) collective-permute-start(bf16[128]{0:T(256)(128)(2,1)S(1)} %slice.57), channel_id=1, source_target_pairs={{0,8},{8,16},{16,24},{24,32},{32,40},{40,48},{48,56},{56,64},{64,7... | collective-permute-start | bytes 776 | tf_op jit(solution)/shard_map/ppermute | solution.py:17
  15.1 37.6 %collective-permute-start.2 = (bf16[128,64]{0,1:T(8,128)(2,1)S(1)}, bf16[128,64]{0,1:T(8,128)(2,1)S(1)}, u32[]{:S(2)}, u32[]{:S(2)}) collective-permute-start(bf16[128,64]{0,1:T(8,128)(2,1)S(1)} %slice.60), channel_id=1, source_target_pairs={{0,8},{8,16},{16,24},{24,32},{32,40},{40,48},{48,56},{56,64},{64,7... | collective-permute-start | bytes 49160 | tf_op jit(solution)/shard_map/ppermute | solution.py:17
  17.8 37.6 %collective-permute-start = (bf16[128,64]{0,1:T(8,128)(2,1)S(1)}, bf16[128,64]{0,1:T(8,128)(2,1)S(1)}, u32[]{:S(2)}, u32[]{:S(2)}) collective-permute-start(bf16[128,64]{0,1:T(8,128)(2,1)S(1)} %slice.53), channel_id=1, source_target_pairs={{0,8},{8,16},{16,24},{24,32},{32,40},{40,48},{48,56},{56,64},{64,7... | collective-permute-start | bytes 49160 | tf_op jit(solution)/shard_map/ppermute | solution.py:17
  56.4 5.4 %copy-start.5 = (s32[256,2]{0,1:T(2,128)S(1)}, s32[256,2]{0,1:T(2,128)}, u32[]{:S(2)}) copy-start(s32[256,2]{0,1:T(2,128)} %param.21) | copy-start | bytes 6148
  57.9 29.3 %all-to-all-start = ((bf16[8,256,256]{2,1,0:T(8,128)(2,1)}), bf16[8,256,256]{2,1,0:T(8,128)(2,1)S(1)}, u32[]{:S(2)}, u32[]{:S(2)}) async-start(bf16[8,256,256]{2,1,0:T(8,128)(2,1)} %bitcast.106), calls=%async_computation | async-start | bytes 2097152 | tf_op jit(solution)/shard_map/all_to_all | solution.py:28
  61.7 163.6 %all-gather.3.cloned.1.call-start = ((), (), s32[]{:S(2)}) async-start(), calls=%async_computation.5 | async-start | bytes 4718592 | tf_op jit(solution)/shard_map/all_gather | solution.py:173
  115.3 61.3 %copy-start.4 = (bf16[2048,128]{1,0:T(8,128)(2,1)S(1)}, bf16[2048,128]{1,0:T(8,128)(2,1)}, u32[]{:S(2)}) copy-start(bf16[2048,128]{1,0:T(8,128)(2,1)} %param.29) | copy-start | bytes 1572868
  151.9 25.2 %copy-start.7 = (bf16[2048,128]{1,0:T(8,128)(2,1)S(1)}, bf16[2048,128]{1,0:T(8,128)(2,1)}, u32[]{:S(2)}) copy-start(bf16[2048,128]{1,0:T(8,128)(2,1)} %param.30) | copy-start | bytes 1572868
  151.9 138.3 %all-gather.5.cloned.1.call-start = ((), (), s32[]{:S(2)}) async-start(), calls=%async_computation.6 | async-start | bytes 2949120 | tf_op jit(solution)/shard_map/all_gather | solution.py:70
  152.1 73.2 %copy-start.2 = (bf16[1,2048,128]{2,1,0:T(8,128)(2,1)S(1)}, bf16[1,2048,128]{2,1,0:T(8,128)(2,1)}, u32[]{:S(2)}) copy-start(bf16[1,2048,128]{2,1,0:T(8,128)(2,1)} %param.26) | copy-start | bytes 1572868
  225.3 3.6 %copy-start.1 = (bf16[32,32,2048]{2,1,0:T(8,128)(2,1)S(1)}, bf16[32,32,2048]{2,1,0:T(8,128)(2,1)}, u32[]{:S(2)}) copy-start(bf16[32,32,2048]{2,1,0:T(8,128)(2,1)} %all-gather.3.cloned.1.call-done) | copy-start | bytes 12582916
  225.3 3.6 %copy-start.8 = (bf16[1,2048,128]{2,1,0:T(8,128)(2,1)S(1)}, bf16[1,2048,128]{2,1,0:T(8,128)(2,1)}, u32[]{:S(2)}) copy-start(bf16[1,2048,128]{2,1,0:T(8,128)(2,1)} %param.27) | copy-start | bytes 1572868
  229.0 61.2 %copy-start.9 = (bf16[1,1024,256]{2,1,0:T(8,128)(2,1)S(1)}, bf16[1,1024,256]{2,1,0:T(8,128)(2,1)}, u32[]{:S(2)}) copy-start(bf16[1,1024,256]{2,1,0:T(8,128)(2,1)} %param.28) | copy-start | bytes 1572868
  231.0 80.6 %copy-start.6 = (f32[256,2]{0,1:T(2,128)S(1)}, f32[256,2]{0,1:T(2,128)}, u32[]{:S(2)}) copy-start(f32[256,2]{0,1:T(2,128)} %param.22) | copy-start | bytes 6148
  293.3 54.6 %copy-start.3 = (bf16[1024,256]{1,0:T(8,128)(2,1)S(1)}, bf16[1024,256]{1,0:T(8,128)(2,1)}, u32[]{:S(2)}) copy-start(bf16[1024,256]{1,0:T(8,128)(2,1)} %param.31) | copy-start | bytes 1572868
  293.3 51.6 %all-to-all-start.4 = ((bf16[32,32,256]{2,1,0:T(8,128)(2,1)}), bf16[32,32,256]{2,1,0:T(8,128)(2,1)S(1)}, u32[]{:S(2)}, u32[]{:S(2)}) async-start(bf16[32,32,256]{2,1,0:T(8,128)(2,1)} %bitcast.25), calls=%async_computation.4 | async-start | bytes 1048576 | tf_op jit(solution)/shard_map/all_to_all | solution.py:182
Sparse Core Ops, SparseCore 0:
  152.0 73.2 all-gather.2
  231.1 59.0 all-gather.4
where the time goes:
time: 358 us; the launch traced here: 357 us
  waiting for transfers between devices  186 us (52%)
  blocking collectives  83.5 us (23%)
  starting transfers between devices  37.3 us (10%)
  local copies, waits for them, and re-layouts  15.8 us (4%)
  between operations  13.8 us (4%)
  matrix products  11.9 us (3%)
  other arithmetic  8.26 us (2%)
    all_gather x1, waiting for transfers between devices, sent_together(): lax.all_gather(both, axis, axis=dim, tiled=True)  59.2 us
    all_to_all x2, blocking collectives, moved_by_axis(): lax.all_to_all(blocks, axes[k], split_axis=k, concat_axis=k, tiled=True)  48 us
    all_gather x1, waiting for transfers between devices, shards(): arrived = lax.all_gather(pieces, 'tp', axis=2, tiled=True)  47.7 us
    all_to_all x1, waiting for transfers between devices, shards(): lax.all_to_all(expert_out.reshape(experts, capacity, col_width), SP, spli...  33.1 us
    ppermute x3, waiting for transfers between devices, passed_along(): lax.ppermute(value, axis, [(source, source + steps) for source in range(l...  26.1 us
    all_to_all x1, blocking collectives, sent_to_all(): lax.all_to_all(jnp.broadcast_to(array[None], (size, *array.shape)), axis,...  24.5 us
    all_to_all x1, waiting for transfers between devices, sent_and_summed(): blocks = lax.all_to_all(split_up(array, dim, size), axis, 0, 0, tiled=True)  19.8 us
    all_to_all x1, starting transfers between devices, shards(): lax.all_to_all(expert_out.reshape(experts, capacity, col_width), SP, spli...  18.3 us
  transfers between devices with their start and end apart: 7, of which 6 were waited for; matrix products, arithmetic and copies ran while one was open for 4% of the time, Pallas kernels for 0%

commit v1 on v0

--- a/solution.py
+++ b/solution.py
@@ -9,6 +9,14 @@
 SP = ("sp_0", "sp_1")
 GRP_SP = ("grp", "sp_0", "sp_1")
 epsilon = 1e-06
+
+
+def tiled_gather(value, axis, dim):
+    size = lax.axis_size(axis)
+    repeats = [size if d == dim else 1 for d in range(value.ndim)]
+    return lax.all_to_all(
+        jnp.tile(value, repeats), axis, split_axis=dim, concat_axis=dim, tiled=True
+    )
 
 
 def passed_along(value, axis, steps):
@@ -170,7 +178,7 @@
     pieces = two_step_exchange(
         outgoing.reshape(experts, capacity, col_width), ("sp_0", "sp_1"), (1, 0), 0, 0
     )
-    arrived = lax.all_gather(pieces, "tp", axis=2, tiled=True)
+    arrived = tiled_gather(pieces, "tp", 2)
     expert_rows = arrived.reshape(-1, model_width)
     gate_pre = jnp.dot(expert_rows, expert_gate[0], preferred_element_type=jnp.float32)
     up_lin = jnp.dot(expert_rows, expert_up[0], preferred_element_type=jnp.float32)

time: 358 us -> 445 us (1.24)
  blocking collectives: 83.5 us -> 22.6 us
  waiting for transfers between devices: 186 us -> 246 us
  local copies, waits for them, and re-layouts: 15.8 us -> 75.4 us
  starting transfers between devices: 37.3 us -> 62.2 us
    all_to_all x0 -> x3, waiting for transfers between devices: none -> 107 us  [the longest x1 84.4 us: tiled_gather(): lax.all_to_all(jnp.tile(value, repeats), axis, split_axis=dim, concat_axi...]
    all_gather x1 -> x0, waiting for transfers between devices: 47.7 us -> none  [shards(): arrived = lax.all_gather(pieces, 'tp', axis=2, tiled=True)]
    all_to_all x2 -> x1, blocking collectives: 48 us -> 11.5 us  [moved_by_axis(): lax.all_to_all(blocks, axes[k], split_axis=k, concat_axis=k, tiled=True)]
    unnamed x22 -> x26, local copies, waits for them, and re-layouts: 0.32 us -> 31.5 us
    all_to_all x0 -> x3, starting transfers between devices: none -> 24.9 us  [the longest x1 13.9 us: moved_by_axis(): lax.all_to_all(blocks, axes[k], split_axis=k, concat_axis=k, tiled=True)]
    all_to_all x1 -> x0, blocking collectives: 24.5 us -> none  [sent_to_all(): lax.all_to_all(jnp.broadcast_to(array[None], (size, *array.shape)), axis,...]
    all_to_all x0 -> x1, local copies, waits for them, and re-layouts: none -> 17.5 us  [tiled_gather(): lax.all_to_all(jnp.tile(value, repeats), axis, split_axis=dim, concat_axi...]
    another operation x2 -> x4, local copies, waits for them, and re-layouts: 0.94 us -> 10 us  [the longest x2 9.09 us: tiled_gather(): jnp.tile(value, repeats)]
  transfers between devices with their start and end apart: 7 -> 9, of which waited for: 6 -> 7; matrix products, arithmetic and copies ran while one was open for 4% -> 10% of each run, Pallas kernels for 0% -> 0%
where the time goes in v1:
time: 445 us; the launch traced here: 443 us
  waiting for transfers between devices  246 us (55%)
  local copies, waits for them, and re-layouts  75.4 us (17%)
  starting transfers between devices  62.2 us (14%)
  blocking collectives  22.6 us (5%)
  matrix products  14.4 us (3%)
  between operations  13.8 us (3%)
  other arithmetic  8.26 us (2%)
    all_to_all x1, waiting for transfers between devices, tiled_gather(): lax.all_to_all(jnp.tile(value, repeats), axis, split_axis=dim, concat_axi...  84.4 us
    all_gather x1, waiting for transfers between devices, sent_together(): lax.all_gather(both, axis, axis=dim, tiled=True)  60.1 us
    all_to_all x1, waiting for transfers between devices, shards(): lax.all_to_all(expert_out.reshape(experts, capacity, col_width), SP, spli...  33.1 us
    unnamed x26, local copies, waits for them, and re-layouts  31.5 us
    ppermute x3, waiting for transfers between devices, passed_along(): lax.ppermute(value, axis, [(source, source + steps) for source in range(l...  26.1 us
    all_to_all x1, waiting for transfers between devices, moved_by_axis(): lax.all_to_all(blocks, axes[k], split_axis=k, concat_axis=k, tiled=True)  22.4 us
    all_to_all x1, waiting for transfers between devices, sent_and_summed(): blocks = lax.all_to_all(split_up(array, dim, size), axis, 0, 0, tiled=True)  19.9 us
    all_to_all x1, starting transfers between devices, shards(): lax.all_to_all(expert_out.reshape(experts, capacity, col_width), SP, spli...  18.2 us
  transfers between devices with their start and end apart: 9, of which 7 were waited for; matrix products, arithmetic and copies ran while one was open for 10% of the time, Pallas kernels for 0%

profile of v1, /device:TPU:65, one launch (start us, length us, event | category | flops | bytes accessed | tf_op | source)
XLA Modules:
  0.0 442.7 jit_solution(1627293416514472309)
XLA Ops:
  6.6 0.7 bitcast_convert_fusion
  7.3 7.1 %collective-permute-start.1 = (bf16[128]{0:T(256)(128)(2,1)S(1)}, bf16[128]{0:T(256)(128)(2,1)S(1)}, u32[]{:S(2)}, u32[]{:S(2)}) collective-permute-start(bf16[128]{0:T(256)(128)(2,1)S(1)} %slice.57), channel_id=1, source_target_pairs={{0,8},{8,16},{16,24},{24,32},{32,40},{40,48},{48,56},{56,64},{64,7... | collective-permute-start | bytes 776 | tf_op jit(solution)/shard_map/ppermute | solution.py:25
  14.4 0.7 slice.60
  15.1 1.9 collective-permute-start.2
  17.0 0.7 slice.53
  17.8 6.1 %collective-permute-start = (bf16[128,64]{0,1:T(8,128)(2,1)S(1)}, bf16[128,64]{0,1:T(8,128)(2,1)S(1)}, u32[]{:S(2)}, u32[]{:S(2)}) collective-permute-start(bf16[128,64]{0,1:T(8,128)(2,1)S(1)} %slice.53), channel_id=1, source_target_pairs={{0,8},{8,16},{16,24},{24,32},{32,40},{40,48},{48,56},{56,64},{64,7... | collective-permute-start | bytes 49160 | tf_op jit(solution)/shard_map/ppermute | solution.py:25
  23.9 0.8 copy_bitcast_fusion
  24.7 0.8 copy_bitcast_fusion.2
  25.5 0.9 reshape.254
  26.4 24.3 %collective-permute-done.1 = bf16[128]{0:T(256)(128)(2,1)S(1)} collective-permute-done((bf16[128]{0:T(256)(128)(2,1)S(1)}, bf16[128]{0:T(256)(128)(2,1)S(1)}, u32[]{:S(2)}, u32[]{:S(2)}) %collective-permute-start.1) | collective-permute-done | bytes 288 | tf_op jit(solution)/shard_map/ppermute | solution.py:25
  50.7 0.1 compare_and_fusion
  50.8 1.9 collective-permute-done.2
  52.7 0.7 copy_bitcast_fusion.1
  53.5 0.3 select_reduce_fusion
  53.7 0.7 broadcast_maximum_fusion
  54.6 0.7 exponential_add_fusion
  55.3 0.7 copy_bitcast_fusion.3
  56.1 0.3 fusion.10
  56.4 0.5 convolution_convert_fusion
  56.9 1.1 copy.100
  57.9 3.8 all-to-all-start
  61.7 0.1 copy.63
  61.8 0.1 eq.47
  62.0 0.1 eq.51
  62.2 0.1 copy.62
  62.3 0.1 mul.82
  62.5 1.2 reduce-window.6
  63.6 0.2 slice_reduce_fusion
  64.0 2.4 scatter_custom_fusion
  66.6 0.8 dynamic_slice.7
  67.3 19.9 %all-to-all-done = bf16[8,256,256]{2,1,0:T(8,128)(2,1)S(1)} async-done(((bf16[8,256,256]{2,1,0:T(8,128)(2,1)}), bf16[8,256,256]{2,1,0:T(8,128)(2,1)S(1)}, u32[]{:S(2)}, u32[]{:S(2)}) %all-to-all-start) | async-done | bytes 1048608 | tf_op jit(solution)/shard_map/all_to_all | solution.py:36
  87.2 0.1 convert_reduce_fusion
  87.4 1.0 fusion.17
  88.4 11.1 %psum.7 = f32[256]{0:T(256)S(1)} all-reduce(f32[256]{0:T(256)S(1)} %get-tuple-element.5), channel_id=1, replica_groups=mesh['grp'=2,'sp_0'=16,'sp_1'=2,'tp'=8] {'tp'}, use_global_device_ids=true, to_apply=%region_8.9 | all-reduce | flops 256 | bytes 2048 | tf_op jit(solution)/shard_map/psum | solution.py:158
  99.6 3.9 gather_fusion
  103.5 0.2 copy_select_fusion
  103.7 11.5 %all_to_all.30 = bf16[16,2,1,32,256]{4,3,0,2,1:T(8,128)(2,1)S(1)} all-to-all(bf16[16,2,1,32,256]{4,3,0,2,1:T(8,128)(2,1)S(1)} %copy_select_fusion), channel_id=1, replica_groups=mesh['grp'=2,'sp_0'=16,'sp_1'=2,'tp'=8] {'sp_1'}, dimensions={1} | all-to-all | bytes 1048576 | tf_op jit(solution)/shard_map/all_to_all | solution.py:62
  115.2 0.8 copy.68
  116.1 13.9 %all-to-all-start.2 = ((bf16[16,2,1,32,256]{4,3,1,2,0:T(8,128)(2,1)}), bf16[16,2,1,32,256]{4,3,1,2,0:T(8,128)(2,1)S(1)}, u32[]{:S(2)}, u32[]{:S(2)}) async-start(bf16[16,2,1,32,256]{4,3,1,2,0:T(8,128)(2,1)} %copy.68), calls=%async_computation.2 | async-start | bytes 1048576 | tf_op jit(solution)/shard_map/all_to_all | solution.py:62
  130.1 22.4 %all-to-all-done.2 = bf16[16,2,1,32,256]{4,3,1,2,0:T(8,128)(2,1)S(1)} async-done(((bf16[16,2,1,32,256]{4,3,1,2,0:T(8,128)(2,1)}), bf16[16,2,1,32,256]{4,3,1,2,0:T(8,128)(2,1)S(1)}, u32[]{:S(2)}, u32[]{:S(2)}) %all-to-all-start.2) | async-done | bytes 524320 | tf_op jit(solution)/shard_map/all_to_all | solution.py:62
  152.5 1.0 broadcast_in_dim.70
  153.6 4.4 %all-to-all-start.4 = ((bf16[8,256,256]{1,2,0:T(8,128)(2,1)}), bf16[8,256,256]{1,2,0:T(8,128)(2,1)}, u32[]{:S(2)}, u32[]{:S(2)}) async-start(bf16[8,256,256]{1,2,0:T(8,128)(2,1)} %broadcast_in_dim.70), calls=%async_computation.4 | async-start | bytes 2097152 | tf_op jit(solution)/shard_map/all_to_all | solution.py:42
  158.0 3.0 copy.69
  161.0 6.1 %tile.11 = bf16[32,32,8,256]{1,0,3,2:T(8,128)(2,1)} broadcast(bf16[32,32,256]{1,0,2:T(8,128)(2,1)S(1)} %copy.69), dimensions={0,1,3} | broadcast | bytes 4718592 | tf_op jit(solution)/shard_map/tile | solution.py:18
  167.1 18.7 %reshape.258 = bf16[8,2,131072]{2,1,0:T(2,128)(2,1)} reshape(bf16[2048,32,32]{2,1,0:T(8,128)(2,1)} %bitcast.110) | data formatting | bytes 8388608
  185.8 6.6 %all-to-all-start.3 = ((bf16[8,2,131072]{2,1,0:T(2,128)(2,1)}), bf16[8,2,131072]{2,1,0:T(2,128)(2,1)}, u32[]{:S(2)}, u32[]{:S(2)}) async-start(bf16[8,2,131072]{2,1,0:T(2,128)(2,1)} %reshape.258), calls=%async_computation.3 | async-start | bytes 8388608 | tf_op jit(solution)/shard_map/all_to_all | solution.py:17
  192.4 0.2 all-gather.2.cloned.1.call-start
  192.7 1.7 fusion.50
  194.4 1.7 fusion.9
  196.1 84.4 %all-to-all-done.3 = bf16[8,2,131072]{2,1,0:T(2,128)(2,1)} async-done(((bf16[8,2,131072]{2,1,0:T(2,128)(2,1)}), bf16[8,2,131072]{2,1,0:T(2,128)(2,1)}, u32[]{:S(2)}, u32[]{:S(2)}) %all-to-all-start.3) | async-done | bytes 4194336 | tf_op jit(solution)/shard_map/all_to_all | solution.py:17
  280.5 12.4 %reshape.259 = bf16[2048,32,32]{2,1,0:T(8,128)(2,1)} reshape(bf16[8,2,131072]{2,1,0:T(2,128)(2,1)} %all-to-all-done.3) | data formatting | bytes 8388608
  292.9 17.5 %copy.70 = bf16[32,32,2048]{2,1,0:T(8,128)(2,1)} copy(bf16[32,32,2048]{1,0,2:T(8,128)(2,1)} %bitcast.111) | data formatting | bytes 8388608 | tf_op jit(solution)/shard_map/all_to_all | solution.py:17
  310.5 3.6 fusion.14
  314.1 1.3 fusion.6
  315.3 0.7 pad_maximum_fusion
  316.2 60.1 %all-gather.2.cloned.1.call-done = bf16[1280,1024]{1,0:T(8,128)(2,1)} async-done(((bf16[1280,128]{1,0:T(8,128)(2,1)}), bf16[1280,1024]{1,0:T(8,128)(2,1)}) %all-gather.2.cloned.1.call-update) | async-done | bytes 2621456 | tf_op jit(solution)/shard_map/all_gather | solution.py:78
  376.3 3.2 fusion.2
  379.5 18.2 %all-to-all-start.5 = ((bf16[32,32,256]{2,1,0:T(8,128)(2,1)}), bf16[32,32,256]{2,1,0:T(8,128)(2,1)S(1)}, u32[]{:S(2)}, u32[]{:S(2)}) async-start(bf16[32,32,256]{2,1,0:T(8,128)(2,1)} %bitcast.26), calls=%async_computation.5 | async-start | bytes 1048576 | tf_op jit(solution)/shard_map/all_to_all | solution.py:190
  397.7 0.1 copy.72
  397.8 33.1 %all-to-all-done.5 = bf16[32,32,256]{2,1,0:T(8,128)(2,1)S(1)} async-done(((bf16[32,32,256]{2,1,0:T(8,128)(2,1)}), bf16[32,32,256]{2,1,0:T(8,128)(2,1)S(1)}, u32[]{:S(2)}, u32[]{:S(2)}) %all-to-all-start.5) | async-done | bytes 524320 | tf_op jit(solution)/shard_map/all_to_all | solution.py:190
  430.9 1.9 gather_fusion.1
  432.9 0.3 reshape.226
  433.2 0.7 multiply_reduce_fusion
  433.9 2.0 fusion.8
  (48 shorter events, 0.9 us)
Async XLA Ops:
  6.5 49.8 %copy-start = (bf16[128,2048]{1,0:T(8,128)(2,1)S(1)}, bf16[128,2048]{1,0:T(8,128)(2,1)}, u32[]{:S(2)}) copy-start(bf16[128,2048]{1,0:T(8,128)(2,1)} %param.24) | copy-start | bytes 1572868
  7.3 43.4 %collective-permute-start.1 = (bf16[128]{0:T(256)(128)(2,1)S(1)}, bf16[128]{0:T(256)(128)(2,1)S(1)}, u32[]{:S(2)}, u32[]{:S(2)}) collective-permute-start(bf16[128]{0:T(256)(128)(2,1)S(1)} %slice.57), channel_id=1, source_target_pairs={{0,8},{8,16},{16,24},{24,32},{32,40},{40,48},{48,56},{56,64},{64,7... | collective-permute-start | bytes 776 | tf_op jit(solution)/shard_map/ppermute | solution.py:25
  15.1 37.6 %collective-permute-start.2 = (bf16[128,64]{0,1:T(8,128)(2,1)S(1)}, bf16[128,64]{0,1:T(8,128)(2,1)S(1)}, u32[]{:S(2)}, u32[]{:S(2)}) collective-permute-start(bf16[128,64]{0,1:T(8,128)(2,1)S(1)} %slice.60), channel_id=1, source_target_pairs={{0,8},{8,16},{16,24},{24,32},{32,40},{40,48},{48,56},{56,64},{64,7... | collective-permute-start | bytes 49160 | tf_op jit(solution)/shard_map/ppermute | solution.py:25
  17.8 37.6 %collective-permute-start = (bf16[128,64]{0,1:T(8,128)(2,1)S(1)}, bf16[128,64]{0,1:T(8,128)(2,1)S(1)}, u32[]{:S(2)}, u32[]{:S(2)}) collective-permute-start(bf16[128,64]{0,1:T(8,128)(2,1)S(1)} %slice.53), channel_id=1, source_target_pairs={{0,8},{8,16},{16,24},{24,32},{32,40},{40,48},{48,56},{56,64},{64,7... | collective-permute-start | bytes 49160 | tf_op jit(solution)/shard_map/ppermute | solution.py:25
  56.1 5.6 %copy-start.6 = (s32[256,2]{0,1:T(2,128)S(1)}, s32[256,2]{0,1:T(2,128)}, u32[]{:S(2)}) copy-start(s32[256,2]{0,1:T(2,128)} %param.21) | copy-start | bytes 6148
  57.9 29.3 %all-to-all-start = ((bf16[8,256,256]{2,1,0:T(8,128)(2,1)}), bf16[8,256,256]{2,1,0:T(8,128)(2,1)S(1)}, u32[]{:S(2)}, u32[]{:S(2)}) async-start(bf16[8,256,256]{2,1,0:T(8,128)(2,1)} %bitcast.109), calls=%async_computation | async-start | bytes 2097152 | tf_op jit(solution)/shard_map/all_to_all | solution.py:36
  116.1 36.5 %all-to-all-start.2 = ((bf16[16,2,1,32,256]{4,3,1,2,0:T(8,128)(2,1)}), bf16[16,2,1,32,256]{4,3,1,2,0:T(8,128)(2,1)S(1)}, u32[]{:S(2)}, u32[]{:S(2)}) async-start(bf16[16,2,1,32,256]{4,3,1,2,0:T(8,128)(2,1)} %copy.68), calls=%async_computation.2 | async-start | bytes 1048576 | tf_op jit(solution)/shard_map/all_to_all | solution.py:62
  153.6 32.3 %all-to-all-start.4 = ((bf16[8,256,256]{1,2,0:T(8,128)(2,1)}), bf16[8,256,256]{1,2,0:T(8,128)(2,1)}, u32[]{:S(2)}, u32[]{:S(2)}) async-start(bf16[8,256,256]{1,2,0:T(8,128)(2,1)} %broadcast_in_dim.70), calls=%async_computation.4 | async-start | bytes 2097152 | tf_op jit(solution)/shard_map/all_to_all | solution.py:42
  185.8 6.8 %copy-start.5 = (bf16[2048,128]{1,0:T(8,128)(2,1)S(1)}, bf16[2048,128]{1,0:T(8,128)(2,1)}, u32[]{:S(2)}) copy-start(bf16[2048,128]{1,0:T(8,128)(2,1)} %param.29) | copy-start | bytes 1572868
  185.8 8.5 %copy-start.8 = (bf16[2048,128]{1,0:T(8,128)(2,1)S(1)}, bf16[2048,128]{1,0:T(8,128)(2,1)}, u32[]{:S(2)}) copy-start(bf16[2048,128]{1,0:T(8,128)(2,1)} %param.30) | copy-start | bytes 1572868
  185.8 94.6 %all-to-all-start.3 = ((bf16[8,2,131072]{2,1,0:T(2,128)(2,1)}), bf16[8,2,131072]{2,1,0:T(2,128)(2,1)}, u32[]{:S(2)}, u32[]{:S(2)}) async-start(bf16[8,2,131072]{2,1,0:T(2,128)(2,1)} %reshape.258), calls=%async_computation.3 | async-start | bytes 8388608 | tf_op jit(solution)/shard_map/all_to_all | solution.py:17
  192.4 183.9 %all-gather.2.cloned.1.call-start = ((), (), s32[]{:S(2)}) async-start(), calls=%async_computation.6 | async-start | bytes 2949120 | tf_op jit(solution)/shard_map/all_gather | solution.py:78
  292.9 17.5 %copy-start.3 = (bf16[1,2048,128]{2,1,0:T(8,128)(2,1)S(1)}, bf16[1,2048,128]{2,1,0:T(8,128)(2,1)}, u32[]{:S(2)}) copy-start(bf16[1,2048,128]{2,1,0:T(8,128)(2,1)} %param.26) | copy-start | bytes 1572868
  310.4 3.6 copy-start.2
  310.4 3.6 copy-start.9
  314.1 62.2 %copy-start.10 = (bf16[1,1024,256]{2,1,0:T(8,128)(2,1)S(1)}, bf16[1,1024,256]{2,1,0:T(8,128)(2,1)}, u32[]{:S(2)}) copy-start(bf16[1,1024,256]{2,1,0:T(8,128)(2,1)} %param.28) | copy-start | bytes 1572868
  315.3 82.3 %copy-start.7 = (f32[256,2]{0,1:T(2,128)S(1)}, f32[256,2]{0,1:T(2,128)}, u32[]{:S(2)}) copy-start(f32[256,2]{0,1:T(2,128)} %param.22) | copy-start | bytes 6148
  316.1 117.7 %copy-start.4 = (bf16[1024,256]{1,0:T(8,128)(2,1)S(1)}, bf16[1024,256]{1,0:T(8,128)(2,1)}, u32[]{:S(2)}) copy-start(bf16[1024,256]{1,0:T(8,128)(2,1)} %param.31) | copy-start | bytes 1572868
  376.3 59.6 %copy-start.1 = (bf16[128,2048]{1,0:T(8,128)(2,1)S(1)}, bf16[128,2048]{1,0:T(8,128)(2,1)}, u32[]{:S(2)}) copy-start(bf16[128,2048]{1,0:T(8,128)(2,1)} %param.24) | copy-start | bytes 1572868
  379.5 51.5 %all-to-all-start.5 = ((bf16[32,32,256]{2,1,0:T(8,128)(2,1)}), bf16[32,32,256]{2,1,0:T(8,128)(2,1)S(1)}, u32[]{:S(2)}, u32[]{:S(2)}) async-start(bf16[32,32,256]{2,1,0:T(8,128)(2,1)} %bitcast.26), calls=%async_computation.5 | async-start | bytes 1048576 | tf_op jit(solution)/shard_map/all_to_all | solution.py:190
Sparse Core Ops, SparseCore 0:
  316.3 59.9 all-gather.1
